TPU v7x, 512 devices: a whole 4x4x16 slice. The times are simulated.
512 devices in a mesh: sp: 64 (over z, y), tp: 8 (over x, core).
Axes of the slice: x: 4, y: 4, z: 16, core: 2. Of those that a mesh axis runs over, the one named last changes fastest.
Arguments:
- layer_input_sequence: bfloat16 [24576, 2048], P('sp', 'tp'), may hold values from -6 to 6
- probe_projection_matrix: bfloat16 [2048, 1024], P(None, 'tp'), may hold values from -0.125 to 0.125
- address_projection_matrix: bfloat16 [2048, 1024], P(None, 'tp'), may hold values from -0.125 to 0.125
- content_projection_matrix: bfloat16 [2048, 1024], P(None, 'tp'), may hold values from -2 to 2
- result_valve_matrix: bfloat16 [2048, 1024], P(None, 'tp'), may hold values from -0.125 to 0.125
- shrink_strength_matrix: bfloat16 [2, 2048, 8], replicated, may hold values from -0.125 to 0.125
- causal_filter_coefficients: bfloat16 [3, 4, 1024], P(None, None, 'tp'), may hold values from -3 to 3
- channel_group_fading_speed: float32 [8], replicated, may hold values from 0 to 0.06, as said below
- summed_shrink_logs: float32 [24576, 8], P('sp', 'tp'), may hold values from -0.7 to 0, as said below
- result_scaling_vector: bfloat16 [128], replicated, may hold values from 0.099609375 to 1.8984375
- generated_probe_vector: bfloat16 [64, 8, 128], P('sp', 'tp'), may hold values from -6 to 6
Outputs:
- mixed: bfloat16 [24576, 1024], P('sp', 'tp')
- cache: bfloat16 [8, 128, 128], P('tp')
- new_read: float32 [64, 8, 128], P('sp', 'tp')
Inputs may be any that keep to these rules, and one draw needn't show every extreme that they name: `channel_group_fading_speed`: positive rates of each head. `summed_shrink_logs`: zero at all but a few positions of each head.
All inputs are finite; a program needn't handle non-finite values.
Results may differ from a plain program's by a relative error of at most 0.0095.
Values may be sent and summed in bfloat16 or wider, within the bound.
A program may use at most 64 MiB of HBM per device.

v0:
```python
import math
import jax
import jax.numpy as jnp
from jax import lax
from jax.sharding import PartitionSpec as P

DK = 128
BLK = 64
CONV = 4
EPS = 1e-06
HIGH = lax.Precision.HIGHEST


def sent_to_all(shard, axis):
    count = lax.axis_size(axis)
    return lax.all_to_all(
        jnp.broadcast_to(shard[None], (count, *shard.shape)), axis, 0, 0, tiled=True
    )


def in_order(pieces, dim):
    dims = list(pieces.shape[1:])
    dims[dim] *= pieces.shape[0]
    return jnp.moveaxis(pieces, 0, dim).reshape(dims)


def gathered_copies(shard, axis, dim):
    pieces = sent_to_all(shard, axis)
    return in_order(pieces, dim)


def shifted(block, axis, distance):
    devices = range(lax.axis_size(axis))
    route = [(i - distance, i) for i in devices if i - distance in devices]
    return lax.ppermute(block, axis, route)


def silu(value):
    return value * jax.nn.sigmoid(value)


def l2_unit(value):
    return value * lax.rsqrt(jnp.sum(value * value, axis=-1, keepdims=True) + EPS)


def block_terms(query, keys, values, fading_exponent, beta):
    heads, length, width = keys.shape
    count = length // BLK

    def split(array):
        return array.reshape((heads, count, BLK) + array.shape[2:])

    query, keys, values, fading_exponent, beta = (
        split(a) for a in (query, keys, values, fading_exponent, beta)
    )
    summed = jnp.cumsum(fading_exponent, axis=-1)
    places = jnp.arange(BLK)
    inclusive = places[:, None] >= places[None, :]
    strict = places[:, None] > places[None, :]
    decay = jnp.exp(jnp.where(inclusive, summed[..., :, None] - summed[..., None, :], -1e30))
    k_beta = keys * beta[..., None]
    a_mat = jnp.where(
        strict, jnp.einsum("hncd,hnsd->hncs", k_beta, keys, precision=HIGH) * decay, 0.0
    )
    eye = jnp.eye(BLK, dtype=jnp.float32)
    t_mat = lax.linalg.triangular_solve(
        eye + a_mat,
        jnp.broadcast_to(eye, a_mat.shape),
        left_side=True,
        lower=True,
        unit_diagonal=True,
    )
    u_part = jnp.einsum("hncs,hnsd->hncd", t_mat, values * beta[..., None], precision=HIGH)
    w_part = jnp.einsum(
        "hncs,hnsd->hncd", t_mat, k_beta * jnp.exp(summed)[..., None], precision=HIGH
    )
    attend = jnp.where(
        inclusive, jnp.einsum("hncd,hnsd->hncs", query, keys, precision=HIGH) * decay, 0.0
    )
    q_dec = query * jnp.exp(summed)[..., None]
    k_dec = keys * jnp.exp(summed[..., -1:] - summed)[..., None]
    g_last = jnp.exp(summed[..., -1])
    return (u_part, w_part, q_dec, k_dec, attend, g_last)


def matmul_heads(left, right):
    return jnp.einsum("hij,hjk->hik", left, right, precision=HIGH)


def on_device(
    layer_input_sequence,
    probe_projection_matrix,
    address_projection_matrix,
    content_projection_matrix,
    result_valve_matrix,
    shrink_strength_matrix,
    causal_filter_coefficients,
    channel_group_fading_speed,
    summed_shrink_logs,
    result_scaling_vector,
    generated_probe_vector,
):
    tok_rows = layer_input_sequence.shape[0]
    local_width = probe_projection_matrix.shape[1]
    head_count = local_width // DK
    prompt_length = tok_rows * lax.axis_size("sp")
    piece = gathered_copies(layer_input_sequence, "tp", 1)
    columns = [
        m
        for m in (
            probe_projection_matrix,
            address_projection_matrix,
            content_projection_matrix,
            result_valve_matrix,
        )
    ]
    projected = jnp.stack([jnp.dot(piece, c, preferred_element_type=jnp.float32) for c in columns])
    rate_terms = jnp.einsum(
        "sd,rdh->srh", piece, shrink_strength_matrix, preferred_element_type=jnp.float32
    )
    projected, rate_terms = (projected, rate_terms)
    raw = projected.astype(jnp.bfloat16)
    rim = shifted(raw[:3, tok_rows - (CONV - 1) :], "sp", 1)
    extended = jnp.concatenate([rim, raw[:3]], axis=1).astype(jnp.float32)
    taps = causal_filter_coefficients.astype(jnp.float32)
    summed_taps = jnp.zeros((3, tok_rows, local_width), jnp.float32)
    for lag in range(CONV):
        summed_taps = summed_taps + taps[:, lag, None, :] * extended[:, lag : lag + tok_rows]
    convolved = silu(summed_taps)
    query = l2_unit(convolved[0].reshape(tok_rows, head_count, DK)) * DK ** (-0.5)
    keys = l2_unit(convolved[1].reshape(tok_rows, head_count, DK))
    values = convolved[2].reshape(tok_rows, head_count, DK)
    first_head = lax.axis_index("tp") * head_count
    diagonal_speed_entries = lax.dynamic_slice_in_dim(rate_terms, first_head, head_count, 2)
    diagonal_fading_multiplier = lax.dynamic_slice_in_dim(
        channel_group_fading_speed, first_head, head_count, 0
    )
    write_shift = math.log(4.0 * prompt_length / DK)
    beta = jax.nn.sigmoid(diagonal_speed_entries[:, 1, :] - write_shift)
    fading_exponent = (
        -diagonal_fading_multiplier[None, :] * jax.nn.softplus(diagonal_speed_entries[:, 0, :])
        + summed_shrink_logs
    )
    terms = block_terms(
        query.transpose(1, 0, 2),
        keys.transpose(1, 0, 2),
        values.transpose(1, 0, 2),
        fading_exponent.T,
        beta.T,
    )
    eye_heads = jnp.broadcast_to(jnp.eye(DK, dtype=jnp.float32), (head_count, DK, DK))
    zero_heads = jnp.zeros((head_count, DK, DK), jnp.float32)

    def local_step(carry, inputs):
        power, offset_state = carry
        u_i, w_i, qd_i, kd_i, a_i, gl_i = inputs
        w_power = jnp.einsum("hcd,hde->hce", w_i, power, precision=HIGH)
        v_zero = u_i - jnp.einsum("hcd,hde->hce", w_i, offset_state, precision=HIGH)
        base = jnp.einsum("hcd,hde->hce", qd_i, offset_state, precision=HIGH) + jnp.einsum(
            "hcs,hse->hce", a_i, v_zero, precision=HIGH
        )
        coupling = jnp.einsum("hcd,hde->hce", qd_i, power, precision=HIGH) - jnp.einsum(
            "hcs,hse->hce", a_i, w_power, precision=HIGH
        )
        power = power * gl_i[:, None, None] - jnp.einsum(
            "hcd,hce->hde", kd_i, w_power, precision=HIGH
        )
        offset_state = offset_state * gl_i[:, None, None] + jnp.einsum(
            "hcd,hce->hde", kd_i, v_zero, precision=HIGH
        )
        return ((power, offset_state), (base, coupling))

    inputs = tuple((jnp.moveaxis(t, 1, 0) for t in terms))
    (power, own_state), (base, coupling) = lax.scan(local_step, (eye_heads, zero_heads), inputs)
    packed = jnp.concatenate([power, own_state], axis=2)[None]
    every_piece = lax.all_gather(packed, "sp", axis=0, tiled=True)

    def walk(carry, piece):
        following = matmul_heads(piece[:, :, :DK], carry) + piece[:, :, DK:]
        return (following, carry)

    final_state, before = lax.scan(walk, zero_heads, every_piece)
    entry_state = lax.dynamic_index_in_dim(before, lax.axis_index("sp"), 0, keepdims=False)
    cache = final_state.astype(jnp.bfloat16)
    outputs = base + jnp.einsum("nhcd,hde->nhce", coupling, entry_state, precision=HIGH)
    heads_out = outputs.transpose(1, 0, 2, 3).reshape(head_count, tok_rows, DK).transpose(1, 0, 2)
    normed = heads_out * lax.rsqrt(jnp.mean(heads_out * heads_out, axis=-1, keepdims=True) + EPS)
    gate_rows = raw[3].reshape(tok_rows, head_count, DK).astype(jnp.float32)
    gated = normed * result_scaling_vector.astype(jnp.float32) * silu(gate_rows)
    mixed = gated.reshape(tok_rows, local_width).astype(jnp.bfloat16)
    unit_query = l2_unit(generated_probe_vector.astype(jnp.float32)) * DK ** (-0.5)
    new_read = jnp.einsum("nhd,hde->nhe", unit_query, cache.astype(jnp.float32), precision=HIGH)
    return (mixed, cache, new_read)


def solution(mesh):
    in_specs = (
        P("sp", "tp"),
        P(None, "tp"),
        P(None, "tp"),
        P(None, "tp"),
        P(None, "tp"),
        P(),
        P(None, None, "tp"),
        P(),
        P("sp", "tp"),
        P(),
        P("sp", "tp", None),
    )
    out_specs = (P("sp", "tp"), P("tp", None, None), P("sp", "tp", None))
    return jax.shard_map(
        on_device, mesh=mesh, in_specs=in_specs, out_specs=out_specs, check_vma=False
    )
```

profile of v0, /device:TPU:2, one launch (start us, length us, event | category | flops | bytes accessed | tf_op | source)
XLA Modules:
  0.0 394.5 jit_solution(7289248820536227078)
XLA Ops:
  7.2 2.3 broadcast_in_dim.65
  9.4 9.5 %all-to-all-start = ((bf16[8,384,256]{2,1,0:T(8,128)(2,1)}), bf16[8,384,256]{2,1,0:T(8,128)(2,1)S(1)}, u32[]{:S(2)}, u32[]{:S(2)}) async-start(bf16[8,384,256]{2,1,0:T(8,128)(2,1)} %broadcast_in_dim.65), calls=%async_computation | async-start | bytes 3145728 | tf_op jit(solution)/shard_map/all_to_all | solution.py:16
  20.4 18.7 %all-to-all-done = bf16[8,384,256]{2,1,0:T(8,128)(2,1)S(1)} async-done(((bf16[8,384,256]{2,1,0:T(8,128)(2,1)}), bf16[8,384,256]{2,1,0:T(8,128)(2,1)S(1)}, u32[]{:S(2)}, u32[]{:S(2)}) %all-to-all-start) | async-done | bytes 1572896 | tf_op jit(solution)/shard_map/all_to_all | solution.py:16
  39.1 1.2 copy-done.1
  40.2 1.6 copy.42
  44.5 1.3 collective-permute-start
  48.5 29.5 %custom-call.3 = f32[1,6,1,64,64]{3,4,2,1,0:T(8,128)S(1)} custom-call(f32[1,6,1,64,64]{4,3,2,1,0:T(8,128)S(1)} %fusion.57), custom_call_target="InvertDiagBlocksLowerTriangular" | custom-call | tf_op jit(solution)/shard_map/triangular_solve | solution.py:66
  80.4 28.9 %while.30 = (s32[]{:T(128)}, f32[1,128,128]{2,1,0:T(8,128)S(1)}, f32[1,128,128]{2,1,0:T(8,128)S(1)}, f32[6,1,64,128]{3,2,1,0:T(8,128)}, f32[6,1,64,128]{3,2,1,0:...) while((s32[]{:T(128)}, f32[1,128,128]{2,1,0:T(8,128)S(1)}, ...), condition=%wide.region_4.5_spmd.clone, body=%wide.region_3.4_spmd.clone.sunk | while | flops 88219648 | bytes 1215665 | solution.py:174
  83.3 0.9 fusion.168
  84.2 1.0 fusion.167
  88.1 0.9 fusion.168
  89.0 1.0 fusion.167
  92.9 0.9 fusion.168
  93.9 1.0 fusion.167
  97.7 0.9 fusion.168
  98.7 1.0 fusion.167
  102.6 0.9 fusion.168
  103.5 1.0 fusion.167
  107.4 0.9 fusion.168
  108.3 1.0 fusion.167
  111.3 157.5 %all-gather.3.cloned.1.call-done = f32[64,128,256]{2,1,0:T(8,128)} async-done(((f32[1,128,256]{2,1,0:T(8,128)}), f32[64,128,256]{2,1,0:T(8,128)}) %all-gather.3.cloned.1.call-update) | async-done | bytes 8388624 | tf_op jit(solution)/shard_map/all_gather | solution.py:176
  268.8 114.5 %while.31 = (s32[]{:T(128)}, f32[1,128,128]{2,1,0:T(8,128)S(1)}, f32[64,1,128,128]{3,2,1,0:T(8,128)}, f32[64,1,128,256]{3,2,1,0:T(8,128)}, s32[]{:T(128)}, /*index=5*/s32[]{:T(128)}) while((s32[]{:T(128)}, f32[1,128,128]{2,1,0:T(8,128)S(1)}, f32[64,1,128,128]{3,2,1,0:T(8,128)}, f32[64,1,128,256]{3,2,1,0:T(8,128)}, s32[]{:T(128)}, ...), condition=%wide.region_6.7_spmd.clone, body=%wide.region_5.6_spmd.clone.sunk | while | flops 25214980 | bytes 787028 | solution.py:182
  269.4 0.9 dynamic-slice_bitcast_fusion.3
  273.0 0.9 dynamic-slice_bitcast_fusion.3
  276.6 0.9 dynamic-slice_bitcast_fusion.3
  278.4 0.9 dynamic-slice_bitcast_fusion.3
  282.0 0.9 dynamic-slice_bitcast_fusion.3
  283.8 0.9 dynamic-slice_bitcast_fusion.3
  285.5 0.9 dynamic-slice_bitcast_fusion.3
  287.3 0.9 dynamic-slice_bitcast_fusion.3
  289.1 0.9 dynamic-slice_bitcast_fusion.3
  294.5 0.9 dynamic-slice_bitcast_fusion.3
  298.1 0.9 dynamic-slice_bitcast_fusion.3
  299.9 0.9 dynamic-slice_bitcast_fusion.3
  301.6 0.9 dynamic-slice_bitcast_fusion.3
  303.4 0.9 dynamic-slice_bitcast_fusion.3
  305.2 0.9 dynamic-slice_bitcast_fusion.3
  307.0 0.9 dynamic-slice_bitcast_fusion.3
  308.8 0.9 dynamic-slice_bitcast_fusion.3
  314.2 0.9 dynamic-slice_bitcast_fusion.3
  316.0 0.9 dynamic-slice_bitcast_fusion.3
  317.8 0.9 dynamic-slice_bitcast_fusion.3
  319.5 0.9 dynamic-slice_bitcast_fusion.3
  321.3 0.9 dynamic-slice_bitcast_fusion.3
  323.1 0.9 dynamic-slice_bitcast_fusion.3
  324.9 0.9 dynamic-slice_bitcast_fusion.3
  383.4 1.2 multiply_reduce_fusion
  385.4 2.3 fusion.69
  (349 shorter events, 117.9 us)
Async XLA Ops:
  7.2 34.7 %copy-start = (bf16[2048,128]{1,0:T(8,128)(2,1)S(1)}, bf16[2048,128]{1,0:T(8,128)(2,1)}, u32[]{:S(2)}) copy-start(bf16[2048,128]{1,0:T(8,128)(2,1)} %param.16) | copy-start | bytes 1572868
  9.4 9.5 %copy-start.11 = (f32[8]{0:T(128)S(1)}, f32[8]{0:T(128)}, u32[]{:S(2)}) copy-start(f32[8]{0:T(128)} %param.22) | copy-start | bytes 100
  9.4 10.8 %copy-start.8 = (bf16[3,4,128]{2,1,0:T(4,128)(2,1)S(1)}, bf16[3,4,128]{2,1,0:T(4,128)(2,1)}, u32[]{:S(2)}) copy-start(bf16[3,4,128]{2,1,0:T(4,128)(2,1)} %param.21) | copy-start | bytes 9220
  9.4 29.6 %all-to-all-start = ((bf16[8,384,256]{2,1,0:T(8,128)(2,1)}), bf16[8,384,256]{2,1,0:T(8,128)(2,1)S(1)}, u32[]{:S(2)}, u32[]{:S(2)}) async-start(bf16[8,384,256]{2,1,0:T(8,128)(2,1)} %broadcast_in_dim.65), calls=%async_computation | async-start | bytes 3145728 | tf_op jit(solution)/shard_map/all_to_all | solution.py:16
  18.9 249.9 %all-gather.3.cloned.1.call-start = ((), (), s32[]{:S(2)}) async-start(), calls=%async_computation.1 | async-start | bytes 8519680 | tf_op jit(solution)/shard_map/all_gather | solution.py:176
  39.1 1.2 copy-start.1
  41.8 1.0 copy-start.2
  42.9 1.0 copy-start.3
  43.9 1.9 copy-start.7
  43.9 2.4 copy-start.9
  44.5 2.6 collective-permute-start
  80.4 29.7 %copy-start.12 = (bf16[128]{0:T(256)(128)(2,1)S(1)}, bf16[128]{0:T(256)(128)(2,1)}, u32[]{:S(2)}) copy-start(bf16[128]{0:T(256)(128)(2,1)} %param.24) | copy-start | bytes 772
  80.4 29.7 %copy-start.10 = (bf16[1,1,128]{2,1,0:T(2,128)(2,1)S(1)}, bf16[1,1,128]{2,1,0:T(2,128)(2,1)}, u32[]{:S(2)}) copy-start(bf16[1,1,128]{2,1,0:T(2,128)(2,1)} %param.25) | copy-start | bytes 772
  268.8 114.5 %copy-start.4 = (f32[6,1,64,128]{3,2,1,0:T(8,128)S(1)}, f32[6,1,64,128]{3,2,1,0:T(8,128)}, u32[]{:S(2)}) copy-start(f32[6,1,64,128]{3,2,1,0:T(8,128)} %get-tuple-element.86) | copy-start | bytes 589828
  268.8 114.6 %copy-start.5 = (f32[6,1,64,128]{3,2,1,0:T(8,128)S(1)}, f32[6,1,64,128]{3,2,1,0:T(8,128)}, u32[]{:S(2)}) copy-start(f32[6,1,64,128]{3,2,1,0:T(8,128)} %get-tuple-element.90) | copy-start | bytes 589828
  384.7 2.9 copy-start.6
Sparse Core Ops, SparseCore 0:
  110.1 158.6 all-gather.2
where the time goes:
time: 396 us; the launch traced here: 394 us
  waiting for transfers between devices  176 us (44%)
  other arithmetic  72.4 us (18%)
  local copies, waits for them, and re-layouts  69.4 us (18%)
  matrix products  47.2 us (12%)
  between operations  15.7 us (4%)
  starting transfers between devices  10.8 us (3%)
    all_gather x1, waiting for transfers between devices, on_device(): every_piece = lax.all_gather(packed, 'sp', axis=0, tiled=True)  157 us
    squeeze x64, local copies, waits for them, and re-layouts, on_device(): final_state, before = lax.scan(walk, zero_heads, every_piece)  58.4 us
    dynamic_update_slice x64, other arithmetic, on_device(): final_state, before = lax.scan(walk, zero_heads, every_piece)  40.2 us
    another operation x4, other arithmetic, block_terms(): lax.linalg.triangular_solve(eye + a_mat, jnp.broadcast_to(eye, a_mat.shap...  29.6 us
    all_to_all x1, waiting for transfers between devices, sent_to_all(): lax.all_to_all(jnp.broadcast_to(shard[None], (count, *shard.shape)), axis...  18.7 us
    dot_general x64, matrix products, matmul_heads(): return jnp.einsum('hij,hjk->hik', left, right, precision=HIGH)  13.2 us
    all_to_all x1, starting transfers between devices, sent_to_all(): lax.all_to_all(jnp.broadcast_to(shard[None], (count, *shard.shape)), axis...  9.5 us
  transfers between devices with their start and end apart: 3, of which 2 were waited for; matrix products, arithmetic and copies ran while one was open for 1% of the time, Pallas kernels for 0%

commit v1 on v0

--- a/solution.py
+++ b/solution.py
@@ -173,7 +173,9 @@
     inputs = tuple((jnp.moveaxis(t, 1, 0) for t in terms))
     (power, own_state), (base, coupling) = lax.scan(local_step, (eye_heads, zero_heads), inputs)
     packed = jnp.concatenate([power, own_state], axis=2)[None]
-    every_piece = lax.all_gather(packed, "sp", axis=0, tiled=True)
+    every_piece = jnp.concatenate(
+        lax.all_to_all(jnp.stack([packed] * lax.axis_size("sp")), "sp", 0, 0), axis=0
+    )
 
     def walk(carry, piece):
         following = matmul_heads(piece[:, :, :DK], carry) + piece[:, :, DK:]

time: 396 us -> 614 us (1.55)
  the two profiles are of different devices: /device:TPU:2 before, /device:TPU:8 now
where the time goes in v1:
time: 614 us; the launch traced here: 612 us
  waiting for transfers between devices  390 us (64%)
  local copies, waits for them, and re-layouts  73.7 us (12%)
  other arithmetic  71.8 us (12%)
  matrix products  46.2 us (8%)
  starting transfers between devices  25.3 us (4%)
    all_to_all x1, waiting for transfers between devices, on_device(): lax.all_to_all(jnp.stack([packed] * lax.axis_size('sp')), 'sp', 0, 0)  367 us
    squeeze x64, local copies, waits for them, and re-layouts, on_device(): final_state, before = lax.scan(walk, zero_heads, every_piece)  58.4 us
    dynamic_update_slice x64, other arithmetic, on_device(): final_state, before = lax.scan(walk, zero_heads, every_piece)  40.3 us
    another operation x4, other arithmetic, block_terms(): lax.linalg.triangular_solve(eye + a_mat, jnp.broadcast_to(eye, a_mat.shap...  29.6 us
    all_to_all x1, waiting for transfers between devices, sent_to_all(): lax.all_to_all(jnp.broadcast_to(shard[None], (count, *shard.shape)), axis...  20.1 us
    all_to_all x1, starting transfers between devices, on_device(): lax.all_to_all(jnp.stack([packed] * lax.axis_size('sp')), 'sp', 0, 0)  17.4 us
    dot_general x64, matrix products, matmul_heads(): return jnp.einsum('hij,hjk->hik', left, right, precision=HIGH)  13.2 us
  transfers between devices with their start and end apart: 3, of which 3 were waited for; matrix products, arithmetic and copies ran while one was open for 0% of the time, Pallas kernels for 0%

profile of v1, /device:TPU:8, one launch (start us, length us, event | category | flops | bytes accessed | tf_op | source)
XLA Modules:
  0.0 612.1 jit_solution(17528359774922078529)
XLA Ops:
  0.6 2.3 broadcast_in_dim.62
  2.9 4.4 all-to-all-start
  8.8 20.1 %all-to-all-done = bf16[8,384,256]{2,1,0:T(8,128)(2,1)S(1)} async-done(((bf16[8,384,256]{2,1,0:T(8,128)(2,1)}), bf16[8,384,256]{2,1,0:T(8,128)(2,1)S(1)}, u32[]{:S(2)}, u32[]{:S(2)}) %all-to-all-start) | async-done | bytes 1572896 | tf_op jit(solution)/shard_map/all_to_all | solution.py:16
  28.9 1.2 copy-done.1
  30.1 1.6 copy.42
  34.4 3.5 collective-permute-start
  39.1 3.1 collective-permute-done
  43.6 29.5 %custom-call.3 = f32[1,6,1,64,64]{3,4,2,1,0:T(8,128)S(1)} custom-call(f32[1,6,1,64,64]{4,3,2,1,0:T(8,128)S(1)} %fusion.57), custom_call_target="InvertDiagBlocksLowerTriangular" | custom-call | tf_op jit(solution)/shard_map/triangular_solve | solution.py:66
  75.4 28.9 %while.30 = (s32[]{:T(128)}, f32[1,128,128]{2,1,0:T(8,128)S(1)}, f32[1,128,128]{2,1,0:T(8,128)S(1)}, f32[6,1,64,128]{3,2,1,0:T(8,128)}, f32[6,1,64,128]{3,2,1,0:...) while((s32[]{:T(128)}, f32[1,128,128]{2,1,0:T(8,128)S(1)}, ...), condition=%wide.region_4.5_spmd.clone, body=%wide.region_3.4_spmd.clone.sunk | while | flops 88219648 | bytes 1215665 | solution.py:174
  78.3 0.9 fusion.168
  79.3 1.0 fusion.167
  83.2 0.9 fusion.168
  84.1 1.0 fusion.167
  88.0 0.9 fusion.168
  88.9 1.0 fusion.167
  92.8 0.9 fusion.168
  93.7 1.0 fusion.167
  97.6 0.9 fusion.168
  98.5 1.0 fusion.167
  102.4 0.9 fusion.168
  103.4 1.0 fusion.167
  104.3 4.2 stack.25
  108.6 17.4 %all-to-all-start.1 = ((f32[64,1,1,128,256]{4,3,2,1,0:T(8,128)}), f32[64,1,1,128,256]{4,3,2,1,0:T(8,128)}, u32[]{:S(2)}, u32[]{:S(2)}) async-start(f32[64,1,1,128,256]{4,3,2,1,0:T(8,128)} %stack.25), calls=%async_computation.1 | async-start | bytes 16777216 | tf_op jit(solution)/shard_map/all_to_all | solution.py:177
  127.3 366.9 %all-to-all-done.1 = f32[64,1,1,128,256]{4,3,2,1,0:T(8,128)} async-done(((f32[64,1,1,128,256]{4,3,2,1,0:T(8,128)}), f32[64,1,1,128,256]{4,3,2,1,0:T(8,128)}, u32[]{:S(2)}, u32[]{:S(2)}) %all-to-all-start.1) | async-done | bytes 8388640 | tf_op jit(solution)/shard_map/all_to_all | solution.py:177
  494.2 114.6 %while.31 = (s32[]{:T(128)}, f32[1,128,128]{2,1,0:T(8,128)S(1)}, f32[64,1,128,128]{3,2,1,0:T(8,128)}, f32[64,1,128,256]{3,2,1,0:T(8,128)}, s32[]{:T(128)}, /*index=5*/s32[]{:T(128)}) while((s32[]{:T(128)}, f32[1,128,128]{2,1,0:T(8,128)S(1)}, f32[64,1,128,128]{3,2,1,0:T(8,128)}, f32[64,1,128,256]{3,2,1,0:T(8,128)}, s32[]{:T(128)}, ...), condition=%wide.region_6.7_spmd.clone, body=%wide.region_5.6_spmd.clone.sunk | while | flops 25214980 | bytes 787028 | solution.py:184
  494.9 0.9 dynamic-slice_bitcast_fusion.3
  498.5 0.9 dynamic-slice_bitcast_fusion.3
  500.3 0.9 dynamic-slice_bitcast_fusion.3
  505.6 0.9 dynamic-slice_bitcast_fusion.3
  509.2 0.9 dynamic-slice_bitcast_fusion.3
  511.0 0.9 dynamic-slice_bitcast_fusion.3
  512.8 0.9 dynamic-slice_bitcast_fusion.3
  516.4 0.9 dynamic-slice_bitcast_fusion.3
  521.8 0.9 dynamic-slice_bitcast_fusion.3
  523.5 0.9 dynamic-slice_bitcast_fusion.3
  525.3 0.9 dynamic-slice_bitcast_fusion.3
  527.1 0.9 dynamic-slice_bitcast_fusion.3
  528.9 0.9 dynamic-slice_bitcast_fusion.3
  530.7 0.9 dynamic-slice_bitcast_fusion.3
  532.5 0.9 dynamic-slice_bitcast_fusion.3
  534.3 0.9 dynamic-slice_bitcast_fusion.3
  537.9 0.9 dynamic-slice_bitcast_fusion.3
  539.7 0.9 dynamic-slice_bitcast_fusion.3
  543.2 0.9 dynamic-slice_bitcast_fusion.3
  548.6 0.9 dynamic-slice_bitcast_fusion.3
  550.4 0.9 dynamic-slice_bitcast_fusion.3
  608.9 1.2 multiply_reduce_fusion
  610.9 1.2 fusion.69
  (351 shorter events, 120.0 us)
Async XLA Ops:
  0.6 31.0 %copy-start = (bf16[2048,128]{1,0:T(8,128)(2,1)S(1)}, bf16[2048,128]{1,0:T(8,128)(2,1)}, u32[]{:S(2)}) copy-start(bf16[2048,128]{1,0:T(8,128)(2,1)} %param.16) | copy-start | bytes 1572868
  2.9 4.5 copy-start.12
  2.9 5.8 copy-start.8
  2.9 26.0 %all-to-all-start = ((bf16[8,384,256]{2,1,0:T(8,128)(2,1)}), bf16[8,384,256]{2,1,0:T(8,128)(2,1)S(1)}, u32[]{:S(2)}, u32[]{:S(2)}) async-start(bf16[8,384,256]{2,1,0:T(8,128)(2,1)} %broadcast_in_dim.62), calls=%async_computation | async-start | bytes 3145728 | tf_op jit(solution)/shard_map/all_to_all | solution.py:16
  28.9 1.2 copy-start.1
  31.7 1.0 copy-start.2
  32.7 1.0 copy-start.3
  33.8 4.1 copy-start.7
  33.8 4.6 copy-start.9
  34.4 7.9 %collective-permute-start = (bf16[3,3,128]{2,1,0:T(4,128)(2,1)S(1)}, bf16[3,3,128]{2,1,0:T(4,128)(2,1)S(1)}, u32[]{:S(2)}, u32[]{:S(2)}) collective-permute-start(bf16[3,3,128]{2,1,0:T(4,128)(2,1)S(1)} %pad_maximum_fusion), channel_id=1, source_target_pairs={{0,8},{8,16},{16,24},{24,32},{32,40},{40,48},{48,56},{56,64},{64,7... | collective-permute-start | bytes 6920 | tf_op jit(solution)/shard_map/ppermute | solution.py:35
  108.6 17.4 %copy-start.13 = (bf16[128]{0:T(256)(128)(2,1)S(1)}, bf16[128]{0:T(256)(128)(2,1)}, u32[]{:S(2)}) copy-start(bf16[128]{0:T(256)(128)(2,1)} %param.24) | copy-start | bytes 772
  108.6 17.4 %copy-start.10 = (bf16[1,1,128]{2,1,0:T(2,128)(2,1)S(1)}, bf16[1,1,128]{2,1,0:T(2,128)(2,1)}, u32[]{:S(2)}) copy-start(bf16[1,1,128]{2,1,0:T(2,128)(2,1)} %param.25) | copy-start | bytes 772
  108.6 385.7 %all-to-all-start.1 = ((f32[64,1,1,128,256]{4,3,2,1,0:T(8,128)}), f32[64,1,1,128,256]{4,3,2,1,0:T(8,128)}, u32[]{:S(2)}, u32[]{:S(2)}) async-start(f32[64,1,1,128,256]{4,3,2,1,0:T(8,128)} %stack.25), calls=%async_computation.1 | async-start | bytes 16777216 | tf_op jit(solution)/shard_map/all_to_all | solution.py:177
  494.2 114.6 %copy-start.4 = (f32[6,1,64,128]{3,2,1,0:T(8,128)S(1)}, f32[6,1,64,128]{3,2,1,0:T(8,128)}, u32[]{:S(2)}) copy-start(f32[6,1,64,128]{3,2,1,0:T(8,128)} %get-tuple-element.86) | copy-start | bytes 589828
  494.2 114.6 %copy-start.5 = (f32[6,1,64,128]{3,2,1,0:T(8,128)S(1)}, f32[6,1,64,128]{3,2,1,0:T(8,128)}, u32[]{:S(2)}) copy-start(f32[6,1,64,128]{3,2,1,0:T(8,128)} %get-tuple-element.90) | copy-start | bytes 589828
  494.2 116.6 %copy-start.11 = (bf16[2048,128]{1,0:T(8,128)(2,1)S(1)}, bf16[2048,128]{1,0:T(8,128)(2,1)}, u32[]{:S(2)}) copy-start(bf16[2048,128]{1,0:T(8,128)(2,1)} %param.19) | copy-start | bytes 1572868
  610.2 1.9 copy-start.6
